TPU v7x, 32 devices: a whole 2x2x4 slice. The times are simulated.
32 devices in a mesh: sp: 8 (over z, y), dp: 4 (over x, core).
Axes of the slice: x: 2, y: 2, z: 4, core: 2. Of those that a mesh axis runs over, the one named last changes fastest.
Arguments:
- cotangent: bfloat16 [4, 2048, 4096], P('dp', 'sp'), may hold values from -6 to 6
- up_pre: bfloat16 [4, 2048, 4096], P('dp', 'sp'), may hold values from -6 to 6
- value_pre: bfloat16 [4, 2048, 4096], P('dp', 'sp'), may hold values from -6 to 6
- spatial_weight: bfloat16 [32, 1024, 1024], P('sp', 'dp'), may hold values from -0.1875 to 0.1875
- spatial_bias: float32 [32, 1024], P('sp'), may hold values from 0.5 to 1.5
- value_gain: float32 [4096], replicated, may hold values from 0.1 to 1.9
Outputs:
- up_grad: bfloat16 [4, 2048, 4096], P('dp', 'sp')
- value_grad: bfloat16 [4, 2048, 4096], P('dp', 'sp')
- weight_grad: float32 [32, 1024, 1024], P('sp', 'dp')
- bias_grad: float32 [32, 1024], P('sp', 'dp')
- gain_grad: float32 [4096], replicated
All inputs are finite; a program needn't handle non-finite values.
Results may differ from a plain program's by a relative error of at most 0.0064.
Values may be sent and summed in bfloat16 or wider, within the bound.
A program may use at most 128 MiB of HBM per device.

v0:
```python
import functools
import math

import jax
import jax.numpy as jnp
from jax import lax
from jax.experimental import pallas as pl
from jax.experimental.pallas import tpu as pltpu
from jax.sharding import PartitionSpec as P

norm_floor = 0.5
root_half = 1.0 / math.sqrt(2.0)
inv_root_tau = 1.0 / math.sqrt(2.0 * math.pi)
MESH = pl.DeviceIdType.MESH
f32 = jnp.float32
bf16 = jnp.bfloat16


def phi(x):
    return 0.5 + 0.5 * lax.erf(x * root_half)


def slope(x):
    return phi(x) + x * jnp.exp(-0.5 * x * x) * inv_root_tau


def drain(ref, sem):
    pltpu.make_async_copy(ref, ref, sem).wait()


def loop(count, body):
    def step(i, carry):
        body(i)
        return carry

    lax.fori_loop(0, count, step, 0)


def kernel(
    S, D, gd, tok, block, blocks, c,
    cot, up, val, w, bias, gain,
    up_o, val_o, wg_o, bg_o, gg_o,
    cot_v, up_v, val_v, gate_s, norm_s, gate_h, norm_h, w_full, back_s, mix_s, back_t, mix_t,
    wg_s, wg_r, act, inv_b, bias_s, bias_r, gain_r, gain_d,
    in_ab, in_v, in_w, w_snd, w_rx, w_rc, w_rr, w_fwd,
    g_snd, g_rcv, v_snd, v_rcv, b_snd, b_rcv, m_snd, m_rcv, wg_snd, wg_rcv,
    bs_snd, bs_rcv, gn_snd, gn_rcv, gx_snd, gx_rcv,
):
    s = lax.axis_index("sp")
    d = lax.axis_index("dp")
    groups = S * gd
    rows = block // D
    per_block = block // tok
    half = D // 2
    twin = d + 1 - 2 * lax.rem(d, 2)
    width = groups * c

    def lanes(i, n):
        return pl.ds(pl.multiple_of(i * n, 128), n)

    def sub(i, n):
        return pl.ds(pl.multiple_of(i * n, n), n)

    my_rows = sub(lax.rem(s, per_block), tok)
    my_cols = lanes(s // per_block, c)

    mid = S // 2

    def order(k):
        far = mid - mid * (s // mid) + lax.rem(s + k, mid)
        near = mid * (s // mid) + lax.rem(s + k + 1 - mid, mid)
        return jnp.where(k < mid, far, near)

    def remote(src, dst, snd, rcv, sp, dp):
        pltpu.make_async_remote_copy(
            src_ref=src, dst_ref=dst, send_sem=snd, recv_sem=rcv,
            device_id=(sp, dp), device_id_type=MESH,
        ).start()

    def fetch(g):
        def one(j):
            n = j * gd + g
            pltpu.make_async_copy(up.at[0, :, lanes(n, c)], up_v.at[n], in_ab.at[g, 0]).start()
            pltpu.make_async_copy(cot.at[0, :, lanes(n, c)], cot_v.at[n], in_ab.at[g, 1]).start()
        loop(S, one)

    barrier = pltpu.get_barrier_semaphore()
    loop(S - 1, lambda k: pl.semaphore_signal(
        barrier, inc=1, device_id=(lax.rem(s + k + 1, S), d), device_id_type=MESH))
    loop(D - 1, lambda k: pl.semaphore_signal(
        barrier, inc=1, device_id=(s, lax.rem(d + k + 1, D)), device_id_type=MESH))
    loop(gd, fetch)
    pl.semaphore_wait(barrier, S + D - 2)

    def send_weights(g):
        mine = w_full.at[g, sub(d, rows)]
        loop(half - 1, lambda k: remote(
            w.at[g], mine, w_snd, w_rx.at[g, k], s, lax.rem(d + 2 * k + 2, D)))
        remote(w.at[g], mine, w_snd, w_rc.at[g], s, twin)

    def gate_group(g):
        drain(up_v.at[pl.ds(0, S)], in_ab.at[g, 0])
        drain(cot_v.at[pl.ds(0, S)], in_ab.at[g, 1])

        def chunk(n):
            x = up_v[n].astype(f32)
            a = (x * phi(x)).astype(bf16)
            return (cot_v[n].astype(f32) * a.astype(f32)).astype(bf16)

        def one(k):
            peer = order(k)
            n = peer * gd + g
            gate_s[n] = chunk(n)
            remote(gate_s.at[n], gate_h.at[g, my_rows, my_cols], g_snd, g_rcv.at[g], peer, d)

        loop(S - 1, one)
        gate_h[g, my_rows, my_cols] = chunk(s * gd + g)

    gate_group(0)
    loop(gd, lambda g: pltpu.make_async_copy(w.at[g], w_full.at[g, sub(d, rows)], in_w.at[g]).start())
    loop(gd, send_weights)
    loop(groups, lambda n: pltpu.make_async_copy(val.at[0, :, lanes(n, c)], val_v.at[n], in_v).start())
    loop(gd - 1, lambda g: gate_group(g + 1))

    drain(val_v, in_v)

    def stat(n, acc):
        x = val_v[n].astype(f32)
        a = x * phi(x)
        act[n] = a
        return acc + a * a

    total = lax.fori_loop(0, groups, stat, jnp.zeros((tok, c), f32))
    mean = jnp.sum(total, axis=1, keepdims=True) / width
    inv_b[...] = jnp.broadcast_to(lax.rsqrt(mean + norm_floor), (tok, c))

    def norm_group(g):
        def chunk(n):
            return (act[n] * inv_b[...] * gain[n]).astype(bf16)

        def one(k):
            peer = order(k)
            n = peer * gd + g
            norm_s[n] = chunk(n)
            remote(norm_s.at[n], norm_h.at[g, my_rows, my_cols], v_snd, v_rcv.at[g], peer, d)

        loop(S - 1, one)
        norm_h[g, my_rows, my_cols] = chunk(s * gd + g)

    loop(gd, norm_group)

    part = block * (S - 1) // S
    tile = min(block, 256)

    def give_back(g, src, dst, snd, rcv, near):
        def one(k):
            peer = order(S - 2 - k if near else k)
            remote(
                src.at[g, sub(lax.rem(peer, per_block), tok), lanes(peer // per_block, c)],
                dst.at[s * gd + g], snd, rcv, peer, d)

        loop(S - 1, one)
        dst[s * gd + g] = src[g, my_rows, my_cols]

    def back_group(g):
        def forward(k):
            came = lax.rem(d + D - 2 * k - 2, D)
            piece = w_full.at[g, sub(came, rows)]
            drain(piece, w_rx.at[g, k])
            remote(piece, piece, w_fwd, w_rr.at[g, k], s, twin)

        loop(half - 1, forward)
        drain(w_full.at[g, pl.ds(0, rows)], w_rc.at[g])
        drain(w_full.at[g, pl.ds(0, rows)], in_w.at[g])
        loop(half - 1, lambda k: drain(w_full.at[g, pl.ds(0, rows)], w_rr.at[g, k]))
        drain(gate_h.at[g, pl.ds(0, part)], g_rcv.at[g])

        def one(t):
            cols = lanes(t, tile)
            y = lax.dot_general(
                w_full[g, :, cols], gate_h[g], (((0,), (0,)), ((), ())), preferred_element_type=f32)
            back_s[g, sub(t, tile), :] = y.astype(bf16)

        loop(block // tile, one)
        give_back(g, back_s, back_t, b_snd, b_rcv, False)
        bias_s[g] = lax.dot_general(
            jnp.ones((8, blocks * c), bf16), gate_h[g], (((1,), (1,)), ((), ())),
            preferred_element_type=f32)

    loop(gd, back_group)
    loop(D - 1, lambda k: remote(
        bias_s.at[:, :, lanes(lax.rem(d + k + 1, D), rows)], bias_r.at[k], bs_snd, bs_rcv,
        s, lax.rem(d + k + 1, D)))

    def mix_group(g):
        drain(norm_h.at[g, pl.ds(0, part)], v_rcv.at[g])

        def grad(peer):
            return lax.dot_general(
                gate_h[g, sub(peer, rows), :], norm_h[g], (((1,), (1,)), ((), ())),
                preferred_element_type=f32)

        def one(k):
            peer = lax.rem(d + k + 1, D)
            wg_s[g, k] = grad(peer).astype(bf16)
            remote(wg_s.at[g, k], wg_r.at[g, k], wg_snd, wg_rcv.at[g], s, peer)

        loop(D - 1, one)

        def mul(t):
            at = sub(t, tile)
            y = jnp.dot(w_full[g, at, :], norm_h[g], preferred_element_type=f32)
            col = jnp.broadcast_to(bias[pl.ds(g, 1), lanes(t, tile)], (c, tile)).T
            mix_s[g, at, :] = (y + jnp.concatenate([col] * blocks, axis=1)).astype(bf16)

        loop(block // tile, mul)
        give_back(g, mix_s, mix_t, m_snd, m_rcv.at[g], True)
        wg_o[g] = grad(d)

    loop(gd, mix_group)

    drain(back_t.at[pl.ds(0, (S - 1) * gd)], b_rcv)

    def dots(n, acc):
        p = back_t[n].astype(f32) * act[n]
        gain_r[s, pl.ds(n, 1), :] = jnp.sum(p * inv_b[...], axis=0, keepdims=True)
        return acc + p * gain[n]

    total = lax.fori_loop(0, groups, dots, jnp.zeros((tok, c), f32))
    loop(S - 1, lambda k: remote(
        gain_r.at[s], gain_r.at[s], gn_snd, gn_rcv, lax.rem(s + k + 1, S), d))
    coef = jnp.sum(total, axis=1, keepdims=True) / width

    def value_out(n):
        inv = inv_b[...]
        scaled = back_t[n].astype(f32) * gain[n]
        y = inv * scaled - inv * inv * inv * act[n] * coef
        val_o[0, :, lanes(n, c)] = (y * slope(val_v[n].astype(f32))).astype(bf16)

    loop(groups, value_out)

    drain(gain_r.at[pl.ds(0, S - 1)], gn_rcv)
    gain_d[d] = lax.fori_loop(
        0, S, lambda k, acc: acc + gain_r[k], jnp.zeros((groups, c), f32))
    loop(D - 1, lambda k: remote(
        gain_d.at[d], gain_d.at[d], gx_snd, gx_rcv, s, lax.rem(d + k + 1, D)))

    drain(bias_r, bs_rcv)
    total = lax.fori_loop(
        0, D - 1, lambda k, acc: acc + bias_r[k], bias_s[:, :, lanes(d, rows)])
    bg_o[...] = total[:, 0, :]

    def up_slope(n):
        act[n] = slope(up_v[n].astype(f32))

    loop(groups, up_slope)

    def sum_weight_grad(g):
        drain(wg_r.at[g], wg_rcv.at[g])

        def one(t):
            at = sub(t, 32)
            acc = wg_o[g, at, :]
            for k in range(D - 1):
                acc = acc + wg_r[g, k, at, :].astype(f32)
            wg_o[g, at, :] = acc

        loop(rows // 32, one)

    def up_group(g):
        sum_weight_grad(g)
        drain(mix_t.at[pl.ds(0, S - 1)], m_rcv.at[g])

        def one(j):
            n = j * gd + g
            mid = (cot_v[n].astype(f32) * mix_t[n].astype(f32)).astype(bf16)
            up_o[0, :, lanes(n, c)] = (mid.astype(f32) * act[n]).astype(bf16)

        loop(S, one)

    drain(gain_d.at[pl.ds(0, D - 1)], gx_rcv)
    gg_o[...] = lax.fori_loop(
        0, D, lambda k, acc: acc + gain_d[k], jnp.zeros((groups, c), f32))
    drain(gain_r.at[pl.ds(0, S - 1)], gn_snd)

    loop(gd, up_group)

    drain(w_full.at[:, pl.ds(0, half * rows)], w_snd)
    if half > 1:
        drain(w_full.at[:, pl.ds(0, (half - 1) * rows)], w_fwd)
    chunks = pl.ds(0, (S - 1) * gd)
    drain(gate_s.at[chunks], g_snd)
    drain(norm_s.at[chunks], v_snd)
    drain(back_t.at[chunks], b_snd)
    drain(mix_t.at[chunks], m_snd)
    drain(wg_s, wg_snd)
    drain(bias_r, bs_snd)
    drain(gain_d.at[pl.ds(0, D - 1)], gx_snd)


def finish(*refs):
    ins, outs, sems = refs[:5], refs[5:10], refs[10]
    copies = [pltpu.make_async_copy(a, b, sems.at[i]) for i, (a, b) in enumerate(zip(ins, outs))]
    for copy in copies:
        copy.start()
    for copy in copies:
        copy.wait()


def shards(S, D, cotangent, up_pre, value_pre, spatial_weight, spatial_bias, value_gain):
    tok, width = cotangent.shape[1:]
    gd, rows, block = spatial_weight.shape
    groups = gd * S
    c = width // groups
    blocks = tok * S // block
    half = D // 2
    dma = pltpu.SemaphoreType.DMA
    vm = pltpu.VMEM
    tokens = vm((groups, tok, c), bf16)
    heads = vm((gd, block, blocks * c), bf16)
    scratch = [
        tokens, tokens, tokens, tokens, tokens, heads, heads,
        vm((gd, block, block), bf16), heads, heads, tokens, tokens,
        vm((gd, D - 1, rows, block), bf16), vm((gd, D - 1, rows, block), bf16),
        vm((groups, tok, c), f32), vm((tok, c), f32),
        vm((gd, 8, block), f32), vm((D - 1, gd, 8, rows), f32),
        vm((S, groups, c), f32), vm((D, groups, c), f32),
        dma((gd, 2)), dma, dma((gd,)), dma, dma((gd, half)), dma((gd,)), dma((gd, half)), dma,
        dma, dma((gd,)), dma, dma((gd,)), dma, dma, dma, dma((gd,)), dma, dma((gd,)),
        dma, dma, dma, dma, dma, dma,
    ]
    anywhere = pl.BlockSpec(memory_space=pl.ANY)
    local = pl.BlockSpec(memory_space=pltpu.VMEM)
    outs = pl.pallas_call(
        functools.partial(kernel, S, D, gd, tok, block, blocks, c),
        out_shape=(
            vm((1, tok, width), bf16), vm((1, tok, width), bf16), vm((gd, rows, block), f32),
            vm((gd, rows), f32), vm((groups, c), f32),
        ),
        in_specs=[anywhere] * 4 + [local] * 2,
        out_specs=(local,) * 5,
        scratch_shapes=scratch,
        compiler_params=pltpu.CompilerParams(
            collective_id=0, has_side_effects=True, vmem_limit_bytes=55 * 2**20),
    )(
        cotangent, up_pre, value_pre, spatial_weight,
        spatial_bias, value_gain.reshape(groups, 1, c),
    )
    outs = pl.pallas_call(
        finish,
        out_shape=[jax.ShapeDtypeStruct(o.shape, o.dtype) for o in outs],
        in_specs=[anywhere] * 5,
        out_specs=[anywhere] * 5,
        scratch_shapes=[dma((5,))],
        compiler_params=pltpu.CompilerParams(vmem_limit_bytes=2**20),
    )(*outs)
    return (*outs[:4], outs[4].reshape(width))


def solution(mesh):
    tokens = P("dp", "sp", None)
    return jax.shard_map(
        functools.partial(shards, mesh.shape["sp"], mesh.shape["dp"]),
        mesh=mesh,
        in_specs=(tokens, tokens, tokens, P("sp", "dp", None), P("sp", None), P()),
        out_specs=(tokens, tokens, P("sp", "dp", None), P("sp", "dp"), P()),
        check_vma=False,
    )
```

profile of v0, /device:TPU:0, one launch (start us, length us, event | category | flops | bytes accessed | tf_op | source)
XLA Modules:
  0.0 199.9 jit_solution(15816057855639402797)
XLA Ops:
  0.6 195.8 %shard_map.101 = (bf16[1,256,4096]{2,1,0:T(8,128)(2,1)S(1)}, bf16[1,256,4096]{2,1,0:T(8,128)(2,1)S(1)}, f32[4,256,1024]{2,1,0:T(8,128)S(1)}, f32[4,256]{1,0:T(4,128)S(1)}, f32[32,128]{1,0:T(8,128)S(1)}) custom-call(bf16[1,256,4096]{2,1,0:T(8,128)(2,1)} %cot.1, bf16[1,256,4096]{2,1,0:T(8,128)(2,1)} %up.1, bf16[1,256,4096]{2,1,0:T(8,128)(2,1)} %val.1, ...), custom_call_target="tpu_custom_call" | custom-call | tf_op jit(solution)/shard_map/pallas_call | solution.py:334
  196.5 3.4 %shard_map.102 = (bf16[1,256,4096]{2,1,0:T(8,128)(2,1)}, bf16[1,256,4096]{2,1,0:T(8,128)(2,1)}, f32[4,256,1024]{2,1,0:T(8,128)}, f32[4,256]{1,0:T(4,128)}, f32[32,128]{1,0:T(8,128)}) custom-call(bf16[1,256,4096]{2,1,0:T(8,128)(2,1)S(1)} %get-tuple-element.15.refs_0_, bf16[1,256,4096]{2,1,0:T(8,128)(2,1)S(1)} %get-tuple-element.16.refs_1_, ...), custom_call_target="tpu_custom_call" | custom-call | tf_op jit(solution)/shard_map/pallas_call | solution.py:349
where the time goes:
time: 200 us
  Pallas kernels  199 us (100%)
    pallas_call x1, Pallas kernels, shards(): pl.pallas_call(functools.partial(kernel, S, D, gd, tok, block, blocks, c)...  196 us

commit v1 on v0

--- a/solution.py
+++ b/solution.py
@@ -38,11 +38,11 @@
 
 def kernel(
     S, D, gd, tok, block, blocks, c,
-    cot, up, val, w, bias, gain,
+    cot, up, val, w, bias_in, gain_in,
     up_o, val_o, wg_o, bg_o, gg_o,
     cot_v, up_v, val_v, gate_s, norm_s, gate_h, norm_h, w_full, back_s, mix_s, back_t, mix_t,
-    wg_s, wg_r, act, inv_b, bias_s, bias_r, gain_r, gain_d,
-    in_ab, in_v, in_w, w_snd, w_rx, w_rc, w_rr, w_fwd,
+    wg_s, wg_r, act, inv_b, bias_s, bias_r, gain_all, gain_d, bias, gain,
+    in_ab, in_v, in_w, in_p, w_snd, w_rx, w_rc, w_rr, w_fwd,
     g_snd, g_rcv, v_snd, v_rcv, b_snd, b_rcv, m_snd, m_rcv, wg_snd, wg_rcv,
     bs_snd, bs_rcv, gn_snd, gn_rcv, gx_snd, gx_rcv,
 ):
@@ -119,10 +119,14 @@
     gate_group(0)
     loop(gd, lambda g: pltpu.make_async_copy(w.at[g], w_full.at[g, sub(d, rows)], in_w.at[g]).start())
     loop(gd, send_weights)
+    pltpu.make_async_copy(bias_in, bias, in_p.at[0]).start()
+    pltpu.make_async_copy(gain_in, gain, in_p.at[1]).start()
     loop(groups, lambda n: pltpu.make_async_copy(val.at[0, :, lanes(n, c)], val_v.at[n], in_v).start())
     loop(gd - 1, lambda g: gate_group(g + 1))
 
     drain(val_v, in_v)
+    drain(bias, in_p.at[0])
+    drain(gain, in_p.at[1])
 
     def stat(n, acc):
         x = val_v[n].astype(f32)
@@ -194,6 +198,18 @@
 
     def mix_group(g):
         drain(norm_h.at[g, pl.ds(0, part)], v_rcv.at[g])
+        n = s * gd + g
+
+        def dot(t, acc):
+            at = sub(t, 32)
+            return acc + back_s[g, at, :].astype(f32) * norm_h[g, at, :].astype(f32)
+
+        total = lax.fori_loop(0, block // 32, dot, jnp.zeros((32, blocks * c), f32))
+        total = jnp.sum(total, axis=0, keepdims=True)
+        total = sum(total[:, b * c:(b + 1) * c] for b in range(blocks))
+        gain_d[g, d] = total / gain[n]
+        loop(D - 1, lambda k: remote(
+            gain_d.at[g, d], gain_d.at[g, d], gx_snd, gx_rcv.at[g], s, lax.rem(d + k + 1, D)))
 
         def grad(peer):
             return lax.dot_general(
@@ -214,6 +230,11 @@
             mix_s[g, at, :] = (y + jnp.concatenate([col] * blocks, axis=1)).astype(bf16)
 
         loop(block // tile, mul)
+        drain(gain_d.at[g, pl.ds(0, D - 1)], gx_rcv.at[g])
+        gain_all[n] = lax.fori_loop(
+            0, D, lambda k, acc: acc + gain_d[g, k], jnp.zeros((1, c), f32))
+        loop(S - 1, lambda k: remote(
+            gain_all.at[n], gain_all.at[n], gn_snd, gn_rcv, order(k), d))
         give_back(g, mix_s, mix_t, m_snd, m_rcv.at[g], True)
         wg_o[g] = grad(d)
 
@@ -222,13 +243,9 @@
     drain(back_t.at[pl.ds(0, (S - 1) * gd)], b_rcv)
 
     def dots(n, acc):
-        p = back_t[n].astype(f32) * act[n]
-        gain_r[s, pl.ds(n, 1), :] = jnp.sum(p * inv_b[...], axis=0, keepdims=True)
-        return acc + p * gain[n]
+        return acc + back_t[n].astype(f32) * act[n] * gain[n]
 
     total = lax.fori_loop(0, groups, dots, jnp.zeros((tok, c), f32))
-    loop(S - 1, lambda k: remote(
-        gain_r.at[s], gain_r.at[s], gn_snd, gn_rcv, lax.rem(s + k + 1, S), d))
     coef = jnp.sum(total, axis=1, keepdims=True) / width
 
     def value_out(n):
@@ -238,12 +255,6 @@
         val_o[0, :, lanes(n, c)] = (y * slope(val_v[n].astype(f32))).astype(bf16)
 
     loop(groups, value_out)
-
-    drain(gain_r.at[pl.ds(0, S - 1)], gn_rcv)
-    gain_d[d] = lax.fori_loop(
-        0, S, lambda k, acc: acc + gain_r[k], jnp.zeros((groups, c), f32))
-    loop(D - 1, lambda k: remote(
-        gain_d.at[d], gain_d.at[d], gx_snd, gx_rcv, s, lax.rem(d + k + 1, D)))
 
     drain(bias_r, bs_rcv)
     total = lax.fori_loop(
@@ -267,8 +278,9 @@
 
         loop(rows // 32, one)
 
+    loop(gd, sum_weight_grad)
+
     def up_group(g):
-        sum_weight_grad(g)
         drain(mix_t.at[pl.ds(0, S - 1)], m_rcv.at[g])
 
         def one(j):
@@ -278,24 +290,22 @@
 
         loop(S, one)
 
-    drain(gain_d.at[pl.ds(0, D - 1)], gx_rcv)
-    gg_o[...] = lax.fori_loop(
-        0, D, lambda k, acc: acc + gain_d[k], jnp.zeros((groups, c), f32))
-    drain(gain_r.at[pl.ds(0, S - 1)], gn_snd)
-
     loop(gd, up_group)
+    chunks = pl.ds(0, (S - 1) * gd)
+    drain(gain_all.at[chunks], gn_rcv)
+    gg_o[...] = gain_all[...]
 
     drain(w_full.at[:, pl.ds(0, half * rows)], w_snd)
     if half > 1:
         drain(w_full.at[:, pl.ds(0, (half - 1) * rows)], w_fwd)
-    chunks = pl.ds(0, (S - 1) * gd)
     drain(gate_s.at[chunks], g_snd)
     drain(norm_s.at[chunks], v_snd)
     drain(back_t.at[chunks], b_snd)
     drain(mix_t.at[chunks], m_snd)
     drain(wg_s, wg_snd)
     drain(bias_r, bs_snd)
-    drain(gain_d.at[pl.ds(0, D - 1)], gx_snd)
+    drain(gain_d.at[:, pl.ds(0, D - 1)], gx_snd)
+    drain(gain_all.at[chunks], gn_snd)
 
 
 def finish(*refs):
@@ -324,10 +334,10 @@
         vm((gd, D - 1, rows, block), bf16), vm((gd, D - 1, rows, block), bf16),
         vm((groups, tok, c), f32), vm((tok, c), f32),
         vm((gd, 8, block), f32), vm((D - 1, gd, 8, rows), f32),
-        vm((S, groups, c), f32), vm((D, groups, c), f32),
-        dma((gd, 2)), dma, dma((gd,)), dma, dma((gd, half)), dma((gd,)), dma((gd, half)), dma,
+        vm((groups, 1, c), f32), vm((gd, D, 1, c), f32), vm((gd, block), f32), vm((groups, 1, c), f32),
+        dma((gd, 2)), dma, dma((gd,)), dma((2,)), dma, dma((gd, half)), dma((gd,)), dma((gd, half)), dma,
         dma, dma((gd,)), dma, dma((gd,)), dma, dma, dma, dma((gd,)), dma, dma((gd,)),
-        dma, dma, dma, dma, dma, dma,
+        dma, dma, dma, dma, dma, dma((gd,)),
     ]
     anywhere = pl.BlockSpec(memory_space=pl.ANY)
     local = pl.BlockSpec(memory_space=pltpu.VMEM)
@@ -335,9 +345,9 @@
         functools.partial(kernel, S, D, gd, tok, block, blocks, c),
         out_shape=(
             vm((1, tok, width), bf16), vm((1, tok, width), bf16), vm((gd, rows, block), f32),
-            vm((gd, rows), f32), vm((groups, c), f32),
+            vm((gd, rows), f32), vm((groups, 1, c), f32),
         ),
-        in_specs=[anywhere] * 4 + [local] * 2,
+        in_specs=[anywhere] * 6,
         out_specs=(local,) * 5,
         scratch_shapes=scratch,
         compiler_params=pltpu.CompilerParams(

time: 200 us -> 193 us (0.965)
  Pallas kernels: 199 us -> 192 us
    pallas_call x1, Pallas kernels: 196 us -> 188 us  [shards(): pl.pallas_call(functools.partial(kernel, S, D, gd, tok, block, blocks, c)...]
where the time goes in v1:
time: 193 us
  Pallas kernels  192 us (99%)
    pallas_call x1, Pallas kernels, shards(): pl.pallas_call(functools.partial(kernel, S, D, gd, tok, block, blocks, c)...  188 us

profile of v1, /device:TPU:0, one launch (start us, length us, event | category | flops | bytes accessed | tf_op | source)
XLA Modules:
  0.0 192.6 jit_solution(3600265550627362712)
XLA Ops:
  0.6 188.5 %shard_map.101 = (bf16[1,256,4096]{2,1,0:T(8,128)(2,1)S(1)}, bf16[1,256,4096]{2,1,0:T(8,128)(2,1)S(1)}, f32[4,256,1024]{2,1,0:T(8,128)S(1)}, f32[4,256]{1,0:T(4,128)S(1)}, f32[32,1,128]{2,1,0:T(1,128)S(1)}) custom-call(bf16[1,256,4096]{2,1,0:T(8,128)(2,1)} %cot.1, bf16[1,256,4096]{2,1,0:T(8,128)(2,1)} %up.1, bf16[1,256,4096]{2,1,0:T(8,128)(2,1)} %val.1, ...), custom_call_target="tpu_custom_call" | custom-call | tf_op jit(solution)/shard_map/pallas_call | solution.py:344
  189.1 3.4 %shard_map.102 = (bf16[1,256,4096]{2,1,0:T(8,128)(2,1)}, bf16[1,256,4096]{2,1,0:T(8,128)(2,1)}, f32[4,256,1024]{2,1,0:T(8,128)}, f32[4,256]{1,0:T(4,128)}, f32[32,1,128]{2,1,0:T(1,128)}) custom-call(bf16[1,256,4096]{2,1,0:T(8,128)(2,1)S(1)} %get-tuple-element.15.refs_0_, bf16[1,256,4096]{2,1,0:T(8,128)(2,1)S(1)} %get-tuple-element.16.refs_1_, ...), custom_call_target="tpu_custom_call" | custom-call | tf_op jit(solution)/shard_map/pallas_call | solution.py:359

commit v2 on v1

--- a/solution.py
+++ b/solution.py
@@ -41,9 +41,9 @@
     cot, up, val, w, bias_in, gain_in,
     up_o, val_o, wg_o, bg_o, gg_o,
     cot_v, up_v, val_v, gate_s, norm_s, gate_h, norm_h, w_full, back_s, mix_s, back_t, mix_t,
-    wg_s, wg_r, act, inv_b, bias_s, bias_r, gain_all, gain_d, bias, gain,
+    wg_s, wg_t, wg_f, wg_r, act, inv_b, bias_s, bias_r, gain_all, gain_d, bias, gain,
     in_ab, in_v, in_w, in_p, w_snd, w_rx, w_rc, w_rr, w_fwd,
-    g_snd, g_rcv, v_snd, v_rcv, b_snd, b_rcv, m_snd, m_rcv, wg_snd, wg_rcv,
+    g_snd, g_rcv, v_snd, v_rcv, b_snd, b_rcv, m_snd, m_rcv, wt_snd, wt_rcv, wg_snd, wg_rcv,
     bs_snd, bs_rcv, gn_snd, gn_rcv, gx_snd, gx_rcv,
 ):
     s = lax.axis_index("sp")
@@ -65,11 +65,15 @@
     my_cols = lanes(s // per_block, c)
 
     mid = S // 2
+    quart = S // 4
 
     def order(k):
-        far = mid - mid * (s // mid) + lax.rem(s + k, mid)
+        far = mid - mid * (s // mid) + quart * (k // quart) + lax.rem(s + k, quart)
         near = mid * (s // mid) + lax.rem(s + k + 1 - mid, mid)
         return jnp.where(k < mid, far, near)
+
+    def late_order(k):
+        return order(jnp.where(k < mid - 1, k + mid, k - mid + 1))
 
     def remote(src, dst, snd, rcv, sp, dp):
         pltpu.make_async_remote_copy(
@@ -158,7 +162,7 @@
 
     def give_back(g, src, dst, snd, rcv, near):
         def one(k):
-            peer = order(S - 2 - k if near else k)
+            peer = late_order(k) if near else order(k)
             remote(
                 src.at[g, sub(lax.rem(peer, per_block), tok), lanes(peer // per_block, c)],
                 dst.at[s * gd + g], snd, rcv, peer, d)
@@ -216,12 +220,11 @@
                 gate_h[g, sub(peer, rows), :], norm_h[g], (((1,), (1,)), ((), ())),
                 preferred_element_type=f32)
 
-        def one(k):
-            peer = lax.rem(d + k + 1, D)
-            wg_s[g, k] = grad(peer).astype(bf16)
-            remote(wg_s.at[g, k], wg_r.at[g, k], wg_snd, wg_rcv.at[g], s, peer)
-
-        loop(D - 1, one)
+        def pair(k):
+            wg_s[g, k] = grad(lax.rem(twin + 2 * k + 2, D)).astype(bf16)
+            remote(wg_s.at[g, k], wg_t.at[g, k], wt_snd, wt_rcv.at[g], s, twin)
+
+        loop(half, pair)
 
         def mul(t):
             at = sub(t, tile)
@@ -235,8 +238,16 @@
             0, D, lambda k, acc: acc + gain_d[g, k], jnp.zeros((1, c), f32))
         loop(S - 1, lambda k: remote(
             gain_all.at[n], gain_all.at[n], gn_snd, gn_rcv, order(k), d))
-        give_back(g, mix_s, mix_t, m_snd, m_rcv.at[g], True)
-        wg_o[g] = grad(d)
+        give_back(g, mix_s, mix_t, m_snd, m_rcv.at[n], True)
+        drain(wg_t.at[g], wt_rcv.at[g])
+
+        def across(k):
+            peer = lax.rem(d + 2 * k + 2, D)
+            wg_f[g, k] = (grad(peer) + wg_t[g, k].astype(f32)).astype(bf16)
+            remote(wg_f.at[g, k], wg_r.at[g, k], wg_snd, wg_rcv.at[g], s, peer)
+
+        loop(half - 1, across)
+        wg_o[g] = grad(d) + wg_t[g, half - 1].astype(f32)
 
     loop(gd, mix_group)
 
@@ -267,12 +278,13 @@
     loop(groups, up_slope)
 
     def sum_weight_grad(g):
-        drain(wg_r.at[g], wg_rcv.at[g])
+        if half > 1:
+            drain(wg_r.at[g], wg_rcv.at[g])
 
         def one(t):
             at = sub(t, 32)
             acc = wg_o[g, at, :]
-            for k in range(D - 1):
+            for k in range(half - 1):
                 acc = acc + wg_r[g, k, at, :].astype(f32)
             wg_o[g, at, :] = acc
 
@@ -281,14 +293,17 @@
     loop(gd, sum_weight_grad)
 
     def up_group(g):
-        drain(mix_t.at[pl.ds(0, S - 1)], m_rcv.at[g])
-
-        def one(j):
-            n = j * gd + g
+        def chunk(n):
             mid = (cot_v[n].astype(f32) * mix_t[n].astype(f32)).astype(bf16)
             up_o[0, :, lanes(n, c)] = (mid.astype(f32) * act[n]).astype(bf16)
 
-        loop(S, one)
+        def one(k):
+            n = order(S - 2 - k) * gd + g
+            drain(mix_t.at[n], m_rcv.at[n])
+            chunk(n)
+
+        chunk(s * gd + g)
+        loop(S - 1, one)
 
     loop(gd, up_group)
     chunks = pl.ds(0, (S - 1) * gd)
@@ -302,7 +317,9 @@
     drain(norm_s.at[chunks], v_snd)
     drain(back_t.at[chunks], b_snd)
     drain(mix_t.at[chunks], m_snd)
-    drain(wg_s, wg_snd)
+    drain(wg_s, wt_snd)
+    if half > 1:
+        drain(wg_f, wg_snd)
     drain(bias_r, bs_snd)
     drain(gain_d.at[:, pl.ds(0, D - 1)], gx_snd)
     drain(gain_all.at[chunks], gn_snd)
@@ -310,7 +327,14 @@
 
 def finish(*refs):
     ins, outs, sems = refs[:5], refs[5:10], refs[10]
-    copies = [pltpu.make_async_copy(a, b, sems.at[i]) for i, (a, b) in enumerate(zip(ins, outs))]
+    pairs = []
+    for a, b in zip(ins, outs):
+        parts = min(a.shape[-2], 128) // 32 if a.ndim == 3 else 1
+        size = a.shape[-2] // max(parts, 1)
+        for i in range(max(parts, 1)):
+            at = (slice(None), pl.ds(i * size, size)) if parts > 1 else slice(None)
+            pairs.append((a.at[at], b.at[at]))
+    copies = [pltpu.make_async_copy(a, b, sems.at[i]) for i, (a, b) in enumerate(pairs)]
     for copy in copies:
         copy.start()
     for copy in copies:
@@ -331,12 +355,13 @@
     scratch = [
         tokens, tokens, tokens, tokens, tokens, heads, heads,
         vm((gd, block, block), bf16), heads, heads, tokens, tokens,
-        vm((gd, D - 1, rows, block), bf16), vm((gd, D - 1, rows, block), bf16),
+        vm((gd, half, rows, block), bf16), vm((gd, half, rows, block), bf16),
+        vm((gd, max(half - 1, 1), rows, block), bf16), vm((gd, max(half - 1, 1), rows, block), bf16),
         vm((groups, tok, c), f32), vm((tok, c), f32),
         vm((gd, 8, block), f32), vm((D - 1, gd, 8, rows), f32),
         vm((groups, 1, c), f32), vm((gd, D, 1, c), f32), vm((gd, block), f32), vm((groups, 1, c), f32),
         dma((gd, 2)), dma, dma((gd,)), dma((2,)), dma, dma((gd, half)), dma((gd,)), dma((gd, half)), dma,
-        dma, dma((gd,)), dma, dma((gd,)), dma, dma, dma, dma((gd,)), dma, dma((gd,)),
+        dma, dma((gd,)), dma, dma((gd,)), dma, dma, dma, dma((groups,)), dma, dma((gd,)), dma, dma((gd,)),
         dma, dma, dma, dma, dma, dma((gd,)),
     ]
     anywhere = pl.BlockSpec(memory_space=pl.ANY)
@@ -361,7 +386,7 @@
         out_shape=[jax.ShapeDtypeStruct(o.shape, o.dtype) for o in outs],
         in_specs=[anywhere] * 5,
         out_specs=[anywhere] * 5,
-        scratch_shapes=[dma((5,))],
+        scratch_shapes=[dma((16,))],
         compiler_params=pltpu.CompilerParams(vmem_limit_bytes=2**20),
     )(*outs)
     return (*outs[:4], outs[4].reshape(width))

time: 193 us -> 191 us (0.990)
  Pallas kernels: 192 us -> 190 us
where the time goes in v2:
time: 191 us
  Pallas kernels  190 us (99%)
    pallas_call x1, Pallas kernels, shards(): pl.pallas_call(functools.partial(kernel, S, D, gd, tok, block, blocks, c)...  187 us

profile of v2, /device:TPU:0, one launch (start us, length us, event | category | flops | bytes accessed | tf_op | source)
XLA Modules:
  0.0 190.8 jit_solution(10677306201286135220)
XLA Ops:
  0.6 186.7 %shard_map.101 = (bf16[1,256,4096]{2,1,0:T(8,128)(2,1)S(1)}, bf16[1,256,4096]{2,1,0:T(8,128)(2,1)S(1)}, f32[4,256,1024]{2,1,0:T(8,128)S(1)}, f32[4,256]{1,0:T(4,128)S(1)}, f32[32,1,128]{2,1,0:T(1,128)S(1)}) custom-call(bf16[1,256,4096]{2,1,0:T(8,128)(2,1)} %cot.1, bf16[1,256,4096]{2,1,0:T(8,128)(2,1)} %up.1, bf16[1,256,4096]{2,1,0:T(8,128)(2,1)} %val.1, ...), custom_call_target="tpu_custom_call" | custom-call | tf_op jit(solution)/shard_map/pallas_call | solution.py:369
  187.4 3.4 %shard_map.102 = (bf16[1,256,4096]{2,1,0:T(8,128)(2,1)}, bf16[1,256,4096]{2,1,0:T(8,128)(2,1)}, f32[4,256,1024]{2,1,0:T(8,128)}, f32[4,256]{1,0:T(4,128)}, f32[32,1,128]{2,1,0:T(1,128)}) custom-call(bf16[1,256,4096]{2,1,0:T(8,128)(2,1)S(1)} %get-tuple-element.15.refs_0_, bf16[1,256,4096]{2,1,0:T(8,128)(2,1)S(1)} %get-tuple-element.16.refs_1_, ...), custom_call_target="tpu_custom_call" | custom-call | tf_op jit(solution)/shard_map/pallas_call | solution.py:384

commit v3 on v2

--- a/solution.py
+++ b/solution.py
@@ -42,9 +42,8 @@
     up_o, val_o, wg_o, bg_o, gg_o,
     cot_v, up_v, val_v, gate_s, norm_s, gate_h, norm_h, w_full, back_s, mix_s, back_t, mix_t,
     wg_s, wg_t, wg_f, wg_r, act, inv_b, bias_s, bias_r, gain_all, gain_d, bias, gain,
-    in_ab, in_v, in_w, in_p, w_snd, w_rx, w_rc, w_rr, w_fwd,
-    g_snd, g_rcv, v_snd, v_rcv, b_snd, b_rcv, m_snd, m_rcv, wt_snd, wt_rcv, wg_snd, wg_rcv,
-    bs_snd, bs_rcv, gn_snd, gn_rcv, gx_snd, gx_rcv,
+    in_ab, in_v, w_in, w_rx, sent, g_rcv, v_rcv, b_rcv, m_rcv, wt_rcv, wg_rcv, bs_rcv, gn_rcv, gx_rcv,
+    last_in, near_in,
 ):
     s = lax.axis_index("sp")
     d = lax.axis_index("dp")
@@ -84,53 +83,82 @@
     def fetch(g):
         def one(j):
             n = j * gd + g
-            pltpu.make_async_copy(up.at[0, :, lanes(n, c)], up_v.at[n], in_ab.at[g, 0]).start()
-            pltpu.make_async_copy(cot.at[0, :, lanes(n, c)], cot_v.at[n], in_ab.at[g, 1]).start()
+            pltpu.make_async_copy(up.at[0, :, lanes(n, c)], up_v.at[n], in_ab.at[g]).start()
+            pltpu.make_async_copy(cot.at[0, :, lanes(n, c)], cot_v.at[n], in_ab.at[g]).start()
         loop(S, one)
 
     barrier = pltpu.get_barrier_semaphore()
-    loop(S - 1, lambda k: pl.semaphore_signal(
-        barrier, inc=1, device_id=(lax.rem(s + k + 1, S), d), device_id_type=MESH))
-    loop(D - 1, lambda k: pl.semaphore_signal(
-        barrier, inc=1, device_id=(s, lax.rem(d + k + 1, D)), device_id_type=MESH))
+    low = s < mid
+
+    def signal(sem, sp, dp):
+        pl.semaphore_signal(sem, inc=1, device_id=(sp, dp), device_id_type=MESH)
+
+    @pl.when(s < S - quart)
+    def _():
+        loop(mid, lambda k: signal(barrier, mid - mid * (s // mid) + k, d))
+
+    loop(D - 1, lambda k: signal(barrier, s, lax.rem(d + k + 1, D)))
     loop(gd, fetch)
-    pl.semaphore_wait(barrier, S + D - 2)
+    pl.semaphore_wait(barrier, jnp.where(low, quart, mid) + D - 1)
+
+    @pl.when(s >= S - quart)
+    def _():
+        loop(mid, lambda k: signal(last_in, k, d))
+
+    @pl.when(s >= mid)
+    def _():
+        signal(near_in, s - mid, d)
 
     def send_weights(g):
         mine = w_full.at[g, sub(d, rows)]
         loop(half - 1, lambda k: remote(
-            w.at[g], mine, w_snd, w_rx.at[g, k], s, lax.rem(d + 2 * k + 2, D)))
-        remote(w.at[g], mine, w_snd, w_rc.at[g], s, twin)
-
-    def gate_group(g):
-        drain(up_v.at[pl.ds(0, S)], in_ab.at[g, 0])
-        drain(cot_v.at[pl.ds(0, S)], in_ab.at[g, 1])
-
-        def chunk(n):
-            x = up_v[n].astype(f32)
-            a = (x * phi(x)).astype(bf16)
-            return (cot_v[n].astype(f32) * a.astype(f32)).astype(bf16)
-
-        def one(k):
-            peer = order(k)
-            n = peer * gd + g
-            gate_s[n] = chunk(n)
-            remote(gate_s.at[n], gate_h.at[g, my_rows, my_cols], g_snd, g_rcv.at[g], peer, d)
-
-        loop(S - 1, one)
-        gate_h[g, my_rows, my_cols] = chunk(s * gd + g)
-
-    gate_group(0)
-    loop(gd, lambda g: pltpu.make_async_copy(w.at[g], w_full.at[g, sub(d, rows)], in_w.at[g]).start())
+            w.at[g], mine, sent.at[1], w_rx.at[g], s, lax.rem(d + 2 * k + 2, D)))
+        remote(w.at[g], mine, sent.at[1], w_in.at[g], s, twin)
+
+    def gate_load(g):
+        drain(up_v.at[pl.ds(0, S)], in_ab.at[g])
+        drain(cot_v.at[pl.ds(0, S)], in_ab.at[g])
+
+    def gate_chunk(n):
+        x = up_v[n].astype(f32)
+        a = (x * phi(x)).astype(bf16)
+        return (cot_v[n].astype(f32) * a.astype(f32)).astype(bf16)
+
+    def gate_send(g, k):
+        peer = order(k)
+        n = peer * gd + g
+        gate_s[n] = gate_chunk(n)
+        remote(gate_s.at[n], gate_h.at[g, my_rows, my_cols], sent.at[0], g_rcv.at[g], peer, d)
+
+    def gate_far(g):
+        gate_load(g)
+        loop(mid, lambda k: gate_send(g, k))
+
+    def gate_near(g):
+        loop(mid - 1, lambda k: gate_send(g, k + mid))
+        gate_h[g, my_rows, my_cols] = gate_chunk(s * gd + g)
+
+    gate_load(0)
+    loop(quart, lambda k: gate_send(0, k))
+
+    @pl.when(low)
+    def _():
+        pl.semaphore_wait(last_in, quart)
+        signal(near_in, s + mid, d)
+
+    loop(mid - quart, lambda k: gate_send(0, k + quart))
+    loop(gd, lambda g: pltpu.make_async_copy(w.at[g], w_full.at[g, sub(d, rows)], w_in.at[g]).start())
     loop(gd, send_weights)
-    pltpu.make_async_copy(bias_in, bias, in_p.at[0]).start()
-    pltpu.make_async_copy(gain_in, gain, in_p.at[1]).start()
+    pltpu.make_async_copy(bias_in, bias, in_v).start()
+    pltpu.make_async_copy(gain_in, gain, in_v).start()
     loop(groups, lambda n: pltpu.make_async_copy(val.at[0, :, lanes(n, c)], val_v.at[n], in_v).start())
-    loop(gd - 1, lambda g: gate_group(g + 1))
+    loop(gd - 1, lambda g: gate_far(g + 1))
+    pl.semaphore_wait(near_in, 1)
+    loop(gd, gate_near)
 
     drain(val_v, in_v)
-    drain(bias, in_p.at[0])
-    drain(gain, in_p.at[1])
+    drain(bias, in_v)
+    drain(gain, in_v)
 
     def stat(n, acc):
         x = val_v[n].astype(f32)
@@ -150,7 +178,7 @@
             peer = order(k)
             n = peer * gd + g
             norm_s[n] = chunk(n)
-            remote(norm_s.at[n], norm_h.at[g, my_rows, my_cols], v_snd, v_rcv.at[g], peer, d)
+            remote(norm_s.at[n], norm_h.at[g, my_rows, my_cols], sent.at[0], v_rcv.at[g], peer, d)
 
         loop(S - 1, one)
         norm_h[g, my_rows, my_cols] = chunk(s * gd + g)
@@ -172,15 +200,13 @@
 
     def back_group(g):
         def forward(k):
-            came = lax.rem(d + D - 2 * k - 2, D)
-            piece = w_full.at[g, sub(came, rows)]
-            drain(piece, w_rx.at[g, k])
-            remote(piece, piece, w_fwd, w_rr.at[g, k], s, twin)
-
-        loop(half - 1, forward)
-        drain(w_full.at[g, pl.ds(0, rows)], w_rc.at[g])
-        drain(w_full.at[g, pl.ds(0, rows)], in_w.at[g])
-        loop(half - 1, lambda k: drain(w_full.at[g, pl.ds(0, rows)], w_rr.at[g, k]))
+            piece = w_full.at[g, sub(lax.rem(d + D - 2 * k - 2, D), rows)]
+            remote(piece, piece, sent.at[1], w_in.at[g], s, twin)
+
+        if half > 1:
+            drain(w_full.at[g, pl.ds(0, (half - 1) * rows)], w_rx.at[g])
+            loop(half - 1, forward)
+        drain(w_full.at[g, pl.ds(0, (half + 1) * rows)], w_in.at[g])
         drain(gate_h.at[g, pl.ds(0, part)], g_rcv.at[g])
 
         def one(t):
@@ -190,14 +216,14 @@
             back_s[g, sub(t, tile), :] = y.astype(bf16)
 
         loop(block // tile, one)
-        give_back(g, back_s, back_t, b_snd, b_rcv, False)
+        give_back(g, back_s, back_t, sent.at[0], b_rcv, False)
         bias_s[g] = lax.dot_general(
             jnp.ones((8, blocks * c), bf16), gate_h[g], (((1,), (1,)), ((), ())),
             preferred_element_type=f32)
 
     loop(gd, back_group)
     loop(D - 1, lambda k: remote(
-        bias_s.at[:, :, lanes(lax.rem(d + k + 1, D), rows)], bias_r.at[k], bs_snd, bs_rcv,
+        bias_s.at[:, :, lanes(lax.rem(d + k + 1, D), rows)], bias_r.at[k], sent.at[3], bs_rcv,
         s, lax.rem(d + k + 1, D)))
 
     def mix_group(g):
@@ -213,7 +239,7 @@
         total = sum(total[:, b * c:(b + 1) * c] for b in range(blocks))
         gain_d[g, d] = total / gain[n]
         loop(D - 1, lambda k: remote(
-            gain_d.at[g, d], gain_d.at[g, d], gx_snd, gx_rcv.at[g], s, lax.rem(d + k + 1, D)))
+            gain_d.at[g, d], gain_d.at[g, d], sent.at[3], gx_rcv.at[g], s, lax.rem(d + k + 1, D)))
 
         def grad(peer):
             return lax.dot_general(
@@ -222,7 +248,7 @@
 
         def pair(k):
             wg_s[g, k] = grad(lax.rem(twin + 2 * k + 2, D)).astype(bf16)
-            remote(wg_s.at[g, k], wg_t.at[g, k], wt_snd, wt_rcv.at[g], s, twin)
+            remote(wg_s.at[g, k], wg_t.at[g, k], sent.at[2], wt_rcv.at[g], s, twin)
 
         loop(half, pair)
 
@@ -237,14 +263,14 @@
         gain_all[n] = lax.fori_loop(
             0, D, lambda k, acc: acc + gain_d[g, k], jnp.zeros((1, c), f32))
         loop(S - 1, lambda k: remote(
-            gain_all.at[n], gain_all.at[n], gn_snd, gn_rcv, order(k), d))
-        give_back(g, mix_s, mix_t, m_snd, m_rcv.at[n], True)
+            gain_all.at[n], gain_all.at[n], sent.at[3], gn_rcv, order(k), d))
+        give_back(g, mix_s, mix_t, sent.at[0], m_rcv.at[g], True)
         drain(wg_t.at[g], wt_rcv.at[g])
 
         def across(k):
             peer = lax.rem(d + 2 * k + 2, D)
             wg_f[g, k] = (grad(peer) + wg_t[g, k].astype(f32)).astype(bf16)
-            remote(wg_f.at[g, k], wg_r.at[g, k], wg_snd, wg_rcv.at[g], s, peer)
+            remote(wg_f.at[g, k], wg_r.at[g, k], sent.at[2], wg_rcv.at[g], s, peer)
 
         loop(half - 1, across)
         wg_o[g] = grad(d) + wg_t[g, half - 1].astype(f32)
@@ -293,40 +319,36 @@
     loop(gd, sum_weight_grad)
 
     def up_group(g):
-        def chunk(n):
+        def one(j):
+            n = j * gd + g
             mid = (cot_v[n].astype(f32) * mix_t[n].astype(f32)).astype(bf16)
             up_o[0, :, lanes(n, c)] = (mid.astype(f32) * act[n]).astype(bf16)
 
-        def one(k):
-            n = order(S - 2 - k) * gd + g
-            drain(mix_t.at[n], m_rcv.at[n])
-            chunk(n)
-
-        chunk(s * gd + g)
-        loop(S - 1, one)
+        drain(mix_t.at[pl.ds(0, S - 1)], m_rcv.at[g])
+        loop(S, one)
 
     loop(gd, up_group)
     chunks = pl.ds(0, (S - 1) * gd)
     drain(gain_all.at[chunks], gn_rcv)
     gg_o[...] = gain_all[...]
 
-    drain(w_full.at[:, pl.ds(0, half * rows)], w_snd)
+    drain(w_full.at[:, pl.ds(0, half * rows)], sent.at[1])
     if half > 1:
-        drain(w_full.at[:, pl.ds(0, (half - 1) * rows)], w_fwd)
-    drain(gate_s.at[chunks], g_snd)
-    drain(norm_s.at[chunks], v_snd)
-    drain(back_t.at[chunks], b_snd)
-    drain(mix_t.at[chunks], m_snd)
-    drain(wg_s, wt_snd)
+        drain(w_full.at[:, pl.ds(0, (half - 1) * rows)], sent.at[1])
+    drain(gate_s.at[chunks], sent.at[0])
+    drain(norm_s.at[chunks], sent.at[0])
+    drain(back_t.at[chunks], sent.at[0])
+    drain(mix_t.at[chunks], sent.at[0])
+    drain(wg_s, sent.at[2])
     if half > 1:
-        drain(wg_f, wg_snd)
-    drain(bias_r, bs_snd)
-    drain(gain_d.at[:, pl.ds(0, D - 1)], gx_snd)
-    drain(gain_all.at[chunks], gn_snd)
+        drain(wg_f, sent.at[2])
+    drain(bias_r, sent.at[3])
+    drain(gain_d.at[:, pl.ds(0, D - 1)], sent.at[3])
+    drain(gain_all.at[chunks], sent.at[3])
 
 
 def finish(*refs):
-    ins, outs, sems = refs[:5], refs[5:10], refs[10]
+    ins, outs, sem = refs[:5], refs[5:10], refs[10]
     pairs = []
     for a, b in zip(ins, outs):
         parts = min(a.shape[-2], 128) // 32 if a.ndim == 3 else 1
@@ -334,7 +356,7 @@
         for i in range(max(parts, 1)):
             at = (slice(None), pl.ds(i * size, size)) if parts > 1 else slice(None)
             pairs.append((a.at[at], b.at[at]))
-    copies = [pltpu.make_async_copy(a, b, sems.at[i]) for i, (a, b) in enumerate(pairs)]
+    copies = [pltpu.make_async_copy(a, b, sem) for a, b in pairs]
     for copy in copies:
         copy.start()
     for copy in copies:
@@ -360,9 +382,8 @@
         vm((groups, tok, c), f32), vm((tok, c), f32),
         vm((gd, 8, block), f32), vm((D - 1, gd, 8, rows), f32),
         vm((groups, 1, c), f32), vm((gd, D, 1, c), f32), vm((gd, block), f32), vm((groups, 1, c), f32),
-        dma((gd, 2)), dma, dma((gd,)), dma((2,)), dma, dma((gd, half)), dma((gd,)), dma((gd, half)), dma,
-        dma, dma((gd,)), dma, dma((gd,)), dma, dma, dma, dma((groups,)), dma, dma((gd,)), dma, dma((gd,)),
-        dma, dma, dma, dma, dma, dma((gd,)),
+        dma((gd,)), dma, dma((gd,)), dma((gd,)), dma((4,)), dma((gd,)), dma((gd,)), dma, dma((gd,)),
+        dma((gd,)), dma((gd,)), dma, dma, dma((gd,)), pltpu.SemaphoreType.REGULAR, pltpu.SemaphoreType.REGULAR,
     ]
     anywhere = pl.BlockSpec(memory_space=pl.ANY)
     local = pl.BlockSpec(memory_space=pltpu.VMEM)
@@ -386,7 +407,7 @@
         out_shape=[jax.ShapeDtypeStruct(o.shape, o.dtype) for o in outs],
         in_specs=[anywhere] * 5,
         out_specs=[anywhere] * 5,
-        scratch_shapes=[dma((16,))],
+        scratch_shapes=[dma],
         compiler_params=pltpu.CompilerParams(vmem_limit_bytes=2**20),
     )(*outs)
     return (*outs[:4], outs[4].reshape(width))

time: 191 us -> 191 us (level)
  no operation moved by 1% of the time
where the time goes in v3:
time: 191 us; the launch traced here: 190 us
  Pallas kernels  190 us (99%)
    pallas_call x1, Pallas kernels, shards(): pl.pallas_call(functools.partial(kernel, S, D, gd, tok, block, blocks, c)...  186 us

profile of v3, /device:TPU:0, one launch (start us, length us, event | category | flops | bytes accessed | tf_op | source)
XLA Modules:
  0.0 190.3 jit_solution(3421535780990747140)
XLA Ops:
  0.6 186.4 %shard_map.101 = (bf16[1,256,4096]{2,1,0:T(8,128)(2,1)S(1)}, bf16[1,256,4096]{2,1,0:T(8,128)(2,1)S(1)}, f32[4,256,1024]{2,1,0:T(8,128)S(1)}, f32[4,256]{1,0:T(4,128)S(1)}, f32[32,1,128]{2,1,0:T(1,128)S(1)}) custom-call(bf16[1,256,4096]{2,1,0:T(8,128)(2,1)} %cot.1, bf16[1,256,4096]{2,1,0:T(8,128)(2,1)} %up.1, bf16[1,256,4096]{2,1,0:T(8,128)(2,1)} %val.1, ...), custom_call_target="tpu_custom_call" | custom-call | tf_op jit(solution)/shard_map/pallas_call | solution.py:390
  187.0 3.3 %shard_map.102 = (bf16[1,256,4096]{2,1,0:T(8,128)(2,1)}, bf16[1,256,4096]{2,1,0:T(8,128)(2,1)}, f32[4,256,1024]{2,1,0:T(8,128)}, f32[4,256]{1,0:T(4,128)}, f32[32,1,128]{2,1,0:T(1,128)}) custom-call(bf16[1,256,4096]{2,1,0:T(8,128)(2,1)S(1)} %get-tuple-element.15.refs_0_, bf16[1,256,4096]{2,1,0:T(8,128)(2,1)S(1)} %get-tuple-element.16.refs_1_, ...), custom_call_target="tpu_custom_call" | custom-call | tf_op jit(solution)/shard_map/pallas_call | solution.py:405

commit v4 on v3

--- a/solution.py
+++ b/solution.py
@@ -43,7 +43,7 @@
     cot_v, up_v, val_v, gate_s, norm_s, gate_h, norm_h, w_full, back_s, mix_s, back_t, mix_t,
     wg_s, wg_t, wg_f, wg_r, act, inv_b, bias_s, bias_r, gain_all, gain_d, bias, gain,
     in_ab, in_v, w_in, w_rx, sent, g_rcv, v_rcv, b_rcv, m_rcv, wt_rcv, wg_rcv, bs_rcv, gn_rcv, gx_rcv,
-    last_in, near_in,
+    last_in, near_in, dp_in, in_one,
 ):
     s = lax.axis_index("sp")
     d = lax.axis_index("dp")
@@ -65,6 +65,8 @@
 
     mid = S // 2
     quart = S // 4
+    low = s < mid
+    inner = (s >= quart) & (s < S - quart)
 
     def order(k):
         far = mid - mid * (s // mid) + quart * (k // quart) + lax.rem(s + k, quart)
@@ -80,15 +82,17 @@
             device_id=(sp, dp), device_id_type=MESH,
         ).start()
 
-    def fetch(g):
-        def one(j):
-            n = j * gd + g
-            pltpu.make_async_copy(up.at[0, :, lanes(n, c)], up_v.at[n], in_ab.at[g]).start()
-            pltpu.make_async_copy(cot.at[0, :, lanes(n, c)], cot_v.at[n], in_ab.at[g]).start()
-        loop(S, one)
+    def fetch(n, sem):
+        pltpu.make_async_copy(up.at[0, :, lanes(n, c)], up_v.at[n], sem).start()
+        pltpu.make_async_copy(cot.at[0, :, lanes(n, c)], cot_v.at[n], sem).start()
+
+    def fetched(count, sem):
+        drain(up_v.at[pl.ds(0, count)], sem)
+        drain(cot_v.at[pl.ds(0, count)], sem)
+
+    loop(quart, lambda k: fetch(order(k) * gd, in_one))
 
     barrier = pltpu.get_barrier_semaphore()
-    low = s < mid
 
     def signal(sem, sp, dp):
         pl.semaphore_signal(sem, inc=1, device_id=(sp, dp), device_id_type=MESH)
@@ -97,9 +101,12 @@
     def _():
         loop(mid, lambda k: signal(barrier, mid - mid * (s // mid) + k, d))
 
-    loop(D - 1, lambda k: signal(barrier, s, lax.rem(d + k + 1, D)))
-    loop(gd, fetch)
-    pl.semaphore_wait(barrier, jnp.where(low, quart, mid) + D - 1)
+    loop(D - 1 - d, lambda k: signal(barrier, s, d + k + 1))
+    loop(S - 1 - quart, lambda k: fetch(order(k + quart) * gd, in_ab.at[0]))
+    fetch(s * gd, in_ab.at[0])
+    loop(gd - 1, lambda g: loop(S, lambda j: fetch(j * gd + g + 1, in_ab.at[g + 1])))
+    pl.semaphore_wait(barrier, jnp.where(low, quart, mid) + d)
+    loop(d, lambda k: signal(dp_in, s, k))
 
     @pl.when(s >= S - quart)
     def _():
@@ -115,10 +122,6 @@
             w.at[g], mine, sent.at[1], w_rx.at[g], s, lax.rem(d + 2 * k + 2, D)))
         remote(w.at[g], mine, sent.at[1], w_in.at[g], s, twin)
 
-    def gate_load(g):
-        drain(up_v.at[pl.ds(0, S)], in_ab.at[g])
-        drain(cot_v.at[pl.ds(0, S)], in_ab.at[g])
-
     def gate_chunk(n):
         x = up_v[n].astype(f32)
         a = (x * phi(x)).astype(bf16)
@@ -131,14 +134,14 @@
         remote(gate_s.at[n], gate_h.at[g, my_rows, my_cols], sent.at[0], g_rcv.at[g], peer, d)
 
     def gate_far(g):
-        gate_load(g)
+        fetched(S, in_ab.at[g])
         loop(mid, lambda k: gate_send(g, k))
 
     def gate_near(g):
         loop(mid - 1, lambda k: gate_send(g, k + mid))
         gate_h[g, my_rows, my_cols] = gate_chunk(s * gd + g)
 
-    gate_load(0)
+    fetched(quart, in_one)
     loop(quart, lambda k: gate_send(0, k))
 
     @pl.when(low)
@@ -146,13 +149,19 @@
         pl.semaphore_wait(last_in, quart)
         signal(near_in, s + mid, d)
 
+    fetched(S - quart, in_ab.at[0])
     loop(mid - quart, lambda k: gate_send(0, k + quart))
-    loop(gd, lambda g: pltpu.make_async_copy(w.at[g], w_full.at[g, sub(d, rows)], w_in.at[g]).start())
-    loop(gd, send_weights)
     pltpu.make_async_copy(bias_in, bias, in_v).start()
     pltpu.make_async_copy(gain_in, gain, in_v).start()
     loop(groups, lambda n: pltpu.make_async_copy(val.at[0, :, lanes(n, c)], val_v.at[n], in_v).start())
     loop(gd - 1, lambda g: gate_far(g + 1))
+
+    @pl.when(d < D - 1)
+    def _():
+        pl.semaphore_wait(dp_in, D - 1 - d)
+
+    loop(gd, lambda g: pltpu.make_async_copy(w.at[g], w_full.at[g, sub(d, rows)], w_in.at[g]).start())
+    loop(gd, send_weights)
     pl.semaphore_wait(near_in, 1)
     loop(gd, gate_near)
 
@@ -191,9 +200,10 @@
     def give_back(g, src, dst, snd, rcv, near):
         def one(k):
             peer = late_order(k) if near else order(k)
+            end = jnp.where((g == gd - 1) & inner & (k >= mid - 1), 1, 0) if near else 0
             remote(
                 src.at[g, sub(lax.rem(peer, per_block), tok), lanes(peer // per_block, c)],
-                dst.at[s * gd + g], snd, rcv, peer, d)
+                dst.at[s * gd + g], snd, rcv.at[g + end] if near else rcv, peer, d)
 
         loop(S - 1, one)
         dst[s * gd + g] = src[g, my_rows, my_cols]
@@ -264,13 +274,13 @@
             0, D, lambda k, acc: acc + gain_d[g, k], jnp.zeros((1, c), f32))
         loop(S - 1, lambda k: remote(
             gain_all.at[n], gain_all.at[n], sent.at[3], gn_rcv, order(k), d))
-        give_back(g, mix_s, mix_t, sent.at[0], m_rcv.at[g], True)
+        give_back(g, mix_s, mix_t, sent.at[0], m_rcv, True)
         drain(wg_t.at[g], wt_rcv.at[g])
 
         def across(k):
             peer = lax.rem(d + 2 * k + 2, D)
             wg_f[g, k] = (grad(peer) + wg_t[g, k].astype(f32)).astype(bf16)
-            remote(wg_f.at[g, k], wg_r.at[g, k], sent.at[2], wg_rcv.at[g], s, peer)
+            remote(wg_f.at[g, k], wg_r.at[g, k], sent.at[2], wg_rcv, s, peer)
 
         loop(half - 1, across)
         wg_o[g] = grad(d) + wg_t[g, half - 1].astype(f32)
@@ -304,9 +314,6 @@
     loop(groups, up_slope)
 
     def sum_weight_grad(g):
-        if half > 1:
-            drain(wg_r.at[g], wg_rcv.at[g])
-
         def one(t):
             at = sub(t, 32)
             acc = wg_o[g, at, :]
@@ -316,18 +323,28 @@
 
         loop(rows // 32, one)
 
+    if half > 1:
+        drain(wg_r, wg_rcv)
     loop(gd, sum_weight_grad)
 
+    def up_chunk(g, peer):
+        n = peer * gd + g
+        mid = (cot_v[n].astype(f32) * mix_t[n].astype(f32)).astype(bf16)
+        up_o[0, :, lanes(n, c)] = (mid.astype(f32) * act[n]).astype(bf16)
+
     def up_group(g):
-        def one(j):
-            n = j * gd + g
-            mid = (cot_v[n].astype(f32) * mix_t[n].astype(f32)).astype(bf16)
-            up_o[0, :, lanes(n, c)] = (mid.astype(f32) * act[n]).astype(bf16)
-
         drain(mix_t.at[pl.ds(0, S - 1)], m_rcv.at[g])
-        loop(S, one)
-
-    loop(gd, up_group)
+        loop(S, lambda peer: up_chunk(g, peer))
+
+    inner_far = jnp.where(low, mid, quart)
+    outer_far = jnp.where(low, mid + quart, 0)
+    own = mid * (s // mid)
+    loop(gd - 1, up_group)
+    drain(mix_t.at[pl.ds(0, S - 1 - quart)], m_rcv.at[gd - 1])
+    loop(mid, lambda k: up_chunk(gd - 1, own + k))
+    loop(mid - quart, lambda k: up_chunk(gd - 1, outer_far + k))
+    drain(mix_t.at[pl.ds(0, quart)], m_rcv.at[gd])
+    loop(quart, lambda k: up_chunk(gd - 1, inner_far + k))
     chunks = pl.ds(0, (S - 1) * gd)
     drain(gain_all.at[chunks], gn_rcv)
     gg_o[...] = gain_all[...]
@@ -382,8 +399,9 @@
         vm((groups, tok, c), f32), vm((tok, c), f32),
         vm((gd, 8, block), f32), vm((D - 1, gd, 8, rows), f32),
         vm((groups, 1, c), f32), vm((gd, D, 1, c), f32), vm((gd, block), f32), vm((groups, 1, c), f32),
-        dma((gd,)), dma, dma((gd,)), dma((gd,)), dma((4,)), dma((gd,)), dma((gd,)), dma, dma((gd,)),
-        dma((gd,)), dma((gd,)), dma, dma, dma((gd,)), pltpu.SemaphoreType.REGULAR, pltpu.SemaphoreType.REGULAR,
+        dma((gd,)), dma, dma((gd,)), dma((gd,)), dma((4,)), dma((gd,)), dma((gd,)), dma, dma((gd + 1,)),
+        dma((gd,)), dma, dma, dma, dma((gd,)), pltpu.SemaphoreType.REGULAR, pltpu.SemaphoreType.REGULAR,
+        pltpu.SemaphoreType.REGULAR, dma,
     ]
     anywhere = pl.BlockSpec(memory_space=pl.ANY)
     local = pl.BlockSpec(memory_space=pltpu.VMEM)

time: 191 us -> 190 us (level)
  no operation moved by 1% of the time
where the time goes in v4:
time: 190 us
  Pallas kernels  189 us (99%)
    pallas_call x1, Pallas kernels, shards(): pl.pallas_call(functools.partial(kernel, S, D, gd, tok, block, blocks, c)...  186 us

profile of v4, /device:TPU:0, one launch (start us, length us, event | category | flops | bytes accessed | tf_op | source)
XLA Modules:
  0.0 189.5 jit_solution(17841959705208637454)
XLA Ops:
  0.6 185.6 %shard_map.101 = (bf16[1,256,4096]{2,1,0:T(8,128)(2,1)S(1)}, bf16[1,256,4096]{2,1,0:T(8,128)(2,1)S(1)}, f32[4,256,1024]{2,1,0:T(8,128)S(1)}, f32[4,256]{1,0:T(4,128)S(1)}, f32[32,1,128]{2,1,0:T(1,128)S(1)}) custom-call(bf16[1,256,4096]{2,1,0:T(8,128)(2,1)} %cot.1, bf16[1,256,4096]{2,1,0:T(8,128)(2,1)} %up.1, bf16[1,256,4096]{2,1,0:T(8,128)(2,1)} %val.1, ...), custom_call_target="tpu_custom_call" | custom-call | tf_op jit(solution)/shard_map/pallas_call | solution.py:408
  186.2 3.3 %shard_map.102 = (bf16[1,256,4096]{2,1,0:T(8,128)(2,1)}, bf16[1,256,4096]{2,1,0:T(8,128)(2,1)}, f32[4,256,1024]{2,1,0:T(8,128)}, f32[4,256]{1,0:T(4,128)}, f32[32,1,128]{2,1,0:T(1,128)}) custom-call(bf16[1,256,4096]{2,1,0:T(8,128)(2,1)S(1)} %get-tuple-element.15.refs_0_, bf16[1,256,4096]{2,1,0:T(8,128)(2,1)S(1)} %get-tuple-element.16.refs_1_, ...), custom_call_target="tpu_custom_call" | custom-call | tf_op jit(solution)/shard_map/pallas_call | solution.py:423

commit v5 on v4

--- a/solution.py
+++ b/solution.py
@@ -74,7 +74,7 @@
         return jnp.where(k < mid, far, near)
 
     def late_order(k):
-        return order(jnp.where(k < mid - 1, k + mid, k - mid + 1))
+        return jnp.where(k < mid - 1, order(k + mid), mid - mid * (s // mid) + k - mid + 1)
 
     def remote(src, dst, snd, rcv, sp, dp):
         pltpu.make_async_remote_copy(

time: 190 us -> 188 us (0.989)
  Pallas kernels: 189 us -> 187 us
where the time goes in v5:
time: 188 us
  Pallas kernels  187 us (99%)
    pallas_call x1, Pallas kernels, shards(): pl.pallas_call(functools.partial(kernel, S, D, gd, tok, block, blocks, c)...  184 us

profile of v5, /device:TPU:0, one launch (start us, length us, event | category | flops | bytes accessed | tf_op | source)
XLA Modules:
  0.0 188.1 jit_solution(14362747009686429164)
XLA Ops:
  0.6 184.2 %shard_map.101 = (bf16[1,256,4096]{2,1,0:T(8,128)(2,1)S(1)}, bf16[1,256,4096]{2,1,0:T(8,128)(2,1)S(1)}, f32[4,256,1024]{2,1,0:T(8,128)S(1)}, f32[4,256]{1,0:T(4,128)S(1)}, f32[32,1,128]{2,1,0:T(1,128)S(1)}) custom-call(bf16[1,256,4096]{2,1,0:T(8,128)(2,1)} %cot.1, bf16[1,256,4096]{2,1,0:T(8,128)(2,1)} %up.1, bf16[1,256,4096]{2,1,0:T(8,128)(2,1)} %val.1, ...), custom_call_target="tpu_custom_call" | custom-call | tf_op jit(solution)/shard_map/pallas_call | solution.py:408
  184.8 3.3 %shard_map.102 = (bf16[1,256,4096]{2,1,0:T(8,128)(2,1)}, bf16[1,256,4096]{2,1,0:T(8,128)(2,1)}, f32[4,256,1024]{2,1,0:T(8,128)}, f32[4,256]{1,0:T(4,128)}, f32[32,1,128]{2,1,0:T(1,128)}) custom-call(bf16[1,256,4096]{2,1,0:T(8,128)(2,1)S(1)} %get-tuple-element.15.refs_0_, bf16[1,256,4096]{2,1,0:T(8,128)(2,1)S(1)} %get-tuple-element.16.refs_1_, ...), custom_call_target="tpu_custom_call" | custom-call | tf_op jit(solution)/shard_map/pallas_call | solution.py:423

commit v6 on v4

--- a/solution.py
+++ b/solution.py
@@ -69,7 +69,7 @@
     inner = (s >= quart) & (s < S - quart)
 
     def order(k):
-        far = mid - mid * (s // mid) + quart * (k // quart) + lax.rem(s + k, quart)
+        far = mid - mid * (s // mid) + k
         near = mid * (s // mid) + lax.rem(s + k + 1 - mid, mid)
         return jnp.where(k < mid, far, near)
 

time: 190 us -> 188 us (0.989)
  Pallas kernels: 189 us -> 187 us
where the time goes in v6:
time: 188 us
  Pallas kernels  187 us (99%)
    pallas_call x1, Pallas kernels, shards(): pl.pallas_call(functools.partial(kernel, S, D, gd, tok, block, blocks, c)...  184 us

profile of v6, /device:TPU:0, one launch (start us, length us, event | category | flops | bytes accessed | tf_op | source)
XLA Modules:
  0.0 188.1 jit_solution(14070187912502367890)
XLA Ops:
  0.6 184.2 %shard_map.101 = (bf16[1,256,4096]{2,1,0:T(8,128)(2,1)S(1)}, bf16[1,256,4096]{2,1,0:T(8,128)(2,1)S(1)}, f32[4,256,1024]{2,1,0:T(8,128)S(1)}, f32[4,256]{1,0:T(4,128)S(1)}, f32[32,1,128]{2,1,0:T(1,128)S(1)}) custom-call(bf16[1,256,4096]{2,1,0:T(8,128)(2,1)} %cot.1, bf16[1,256,4096]{2,1,0:T(8,128)(2,1)} %up.1, bf16[1,256,4096]{2,1,0:T(8,128)(2,1)} %val.1, ...), custom_call_target="tpu_custom_call" | custom-call | tf_op jit(solution)/shard_map/pallas_call | solution.py:408
  184.8 3.3 %shard_map.102 = (bf16[1,256,4096]{2,1,0:T(8,128)(2,1)}, bf16[1,256,4096]{2,1,0:T(8,128)(2,1)}, f32[4,256,1024]{2,1,0:T(8,128)}, f32[4,256]{1,0:T(4,128)}, f32[32,1,128]{2,1,0:T(1,128)}) custom-call(bf16[1,256,4096]{2,1,0:T(8,128)(2,1)S(1)} %get-tuple-element.15.refs_0_, bf16[1,256,4096]{2,1,0:T(8,128)(2,1)S(1)} %get-tuple-element.16.refs_1_, ...), custom_call_target="tpu_custom_call" | custom-call | tf_op jit(solution)/shard_map/pallas_call | solution.py:423
